TPU v7x, 32 devices: a whole 2x2x4 slice. The times are simulated.
32 devices in a mesh: sp: 8 (over z, y), tp: 4 (over x, core).
Axes of the slice: x: 2, y: 2, z: 4, core: 2. Of those that a mesh axis runs over, the one named last changes fastest.
Arguments:
- activations: bfloat16 [4096, 2048], P('sp', 'tp'), may hold values from -250 to 250
- norm_gain: bfloat16 [2048], P('tp'), may hold values from 0.099609375 to 1.8984375
- pool_weight: bfloat16 [2048, 1024], P('sp', 'tp'), may hold values from -0.125 to 0.125
- gate_weight: bfloat16 [2048, 1024], P('sp', 'tp'), may hold values from -0.125 to 0.125
- value_weight: bfloat16 [2048, 1024], P('sp', 'tp'), may hold values from -0.125 to 0.125
- key_weight: bfloat16 [2048, 256], P('sp', 'tp'), may hold values from -0.125 to 0.125
- read_weight: bfloat16 [2048, 256], P('sp', 'tp'), may hold values from -0.125 to 0.125
- step_weight: bfloat16 [2048, 16], P('sp', 'tp'), may hold values from -0.125 to 0.125
- pool_mix: bfloat16 [4, 256, 256], P('tp'), may hold values from -0.375 to 0.375
- pool_scale: float32 [1024], P('tp'), may hold values from 0.1 to 1.9
- taps_value: float32 [4, 1024], P(None, 'tp'), may hold values from -3 to 3
- taps_key: float32 [4, 256], P(None, 'tp'), may hold values from -3 to 3
- taps_read: float32 [4, 256], P(None, 'tp'), may hold values from -3 to 3
- step_bias: float32 [16], P('tp'), may hold values from -1 to 1
- decay_log: float32 [16], P('tp')
- decay_extra: float32 [4096, 16], P('sp', 'tp'), may hold values from -1 to 0
- skip_scale: float32 [16], P('tp'), may hold values from 0.5 to 2
- state_gain: float32 [1024], P('tp'), may hold values from 0.1 to 1.9
- out_pool_weight: bfloat16 [1024, 2048], P('tp', 'sp'), may hold values from -0.125 to 0.125
- out_state_weight: bfloat16 [1024, 2048], P('tp', 'sp'), may hold values from -0.125 to 0.125
Outputs:
- mixed: bfloat16 [4096, 2048], P('sp', 'tp')
All inputs are finite; a program needn't handle non-finite values.
Results may differ from a plain program's by a relative error of at most 0.007.
Values may be sent and summed in bfloat16 or wider, within the bound.
A program may use at most 64 MiB of HBM per device.

v0:
```python
import jax
import jax.numpy as jnp
from jax import lax
from jax.sharding import PartitionSpec as P

SSM_STATE = 64
POOL_GROUPS = 4
SCAN_BLOCK = 128
MIX_W = 1024


EPSILON = 1e-06
HIGH = lax.Precision.HIGHEST


def shifted(value, axis, steps):
    count = lax.axis_size(axis)
    leading, last = (max(0, -steps), min(count, count - steps))
    return lax.ppermute(value, axis, [(source, source + steps) for source in range(leading, last)])


def carried_in(part, axis, combine, identity):
    place = lax.axis_index(axis)
    gathered = jax.tree.map(lambda a: lax.all_gather(a, axis), part)
    state = jax.tree.map(lambda a, e: jnp.zeros_like(a) + jnp.asarray(e, a.dtype), part, identity)

    def one(step, state):
        return combine(
            state, jax.tree.map(lambda a: lax.dynamic_index_in_dim(a, step, 0, False), gathered)
        )

    return lax.fori_loop(0, place, one, state)


def backward_kernel(extended, taps):
    width = taps.shape[0]
    length = extended.shape[0] - (width - 1)
    widened_rows = extended.astype(jnp.float32)
    total = jnp.zeros((length, extended.shape[1]), jnp.float32)
    for offset in range(width):
        total = total + taps[offset][None, :] * widened_rows[offset : offset + length]
    return jax.nn.silu(total).astype(jnp.bfloat16)


def combine_states(preceding_token, later):
    return (preceding_token[0] * later[0], preceding_token[1] * later[0][:, None, None] + later[1])


def local(
    activations,
    norm_gain,
    pool_weight,
    gate_weight,
    value_weight,
    key_weight,
    read_weight,
    step_weight,
    pool_mix,
    pool_scale,
    taps_value,
    taps_key,
    taps_read,
    step_bias,
    decay_log,
    decay_extra,
    skip_scale,
    state_gain,
    out_pool_weight,
    out_state_weight,
):
    length = activations.shape[0]
    cluster_span = pool_weight.shape[1]
    local_mix = gate_weight.shape[1]
    local_state = key_weight.shape[1]
    local_heads = step_weight.shape[1]
    joined = jnp.concatenate(
        [pool_weight, gate_weight, value_weight, key_weight, read_weight, step_weight], axis=1
    )
    in_weight = lax.all_gather(joined, "sp", axis=0, tiled=True)
    whole, gains = (
        lax.all_gather(activations, "tp", axis=1, tiled=True),
        lax.all_gather(norm_gain, "tp", axis=0, tiled=True),
    )
    widened_rows = whole.astype(jnp.float32)
    normed = (
        widened_rows
        * lax.rsqrt(jnp.mean(widened_rows * widened_rows, axis=-1, keepdims=True) + EPSILON)
        * gains.astype(jnp.float32)
    ).astype(jnp.bfloat16)
    projected = jnp.dot(normed, in_weight, preferred_element_type=jnp.float32)
    column = 0
    pool_in = projected[:, column : column + cluster_span].astype(jnp.bfloat16)
    column = column + cluster_span
    gate_in = projected[:, column : column + local_mix].astype(jnp.bfloat16)
    column = column + local_mix
    raw_value = projected[:, column : column + local_mix].astype(jnp.bfloat16)
    column = column + local_mix
    raw_key = projected[:, column : column + local_state].astype(jnp.bfloat16)
    column = column + local_state
    raw_read = projected[:, column : column + local_state].astype(jnp.bfloat16)
    column = column + local_state
    step_raw = projected[:, column : column + local_heads]
    raw_joined = jnp.concatenate([raw_value, raw_key, raw_read], axis=1)
    reach = 2**POOL_GROUPS - 1
    width = taps_value.shape[0]
    prior_pool, prior_joined = shifted(
        (pool_in[length - reach :], raw_joined[length - width + 1 :]), "sp", 1
    )
    group = lax.axis_index("tp")
    running = jnp.concatenate([prior_pool, pool_in], axis=0).astype(jnp.float32)
    levels = []
    for level in range(POOL_GROUPS):
        stride = 2**level
        running = running[stride:] + running[:-stride]
        levels.append(running[running.shape[0] - length :])
    window_sum = lax.dynamic_index_in_dim(jnp.stack(levels), group, 0, keepdims=False)
    window = jnp.exp2((group + 1).astype(jnp.float32))
    position = (lax.axis_index("sp") * length + jnp.arange(length, dtype=jnp.int32)).astype(
        jnp.float32
    )
    counts = jnp.minimum(position + 1.0, window)
    pooled = (window_sum / counts[:, None] - pool_in.astype(jnp.float32)).astype(jnp.bfloat16)
    pool_out = (
        jnp.dot(pooled, pool_mix[0], preferred_element_type=jnp.float32) * pool_scale
    ).astype(jnp.bfloat16)
    all_taps = jnp.concatenate([taps_value, taps_key, taps_read], axis=1)
    convolved = backward_kernel(jnp.concatenate([prior_joined, raw_joined], axis=0), all_taps)
    head_value = convolved[:, :local_mix]
    key_vectors = convolved[:, local_mix : local_mix + local_state]
    read_vectors = convolved[:, local_mix + local_state :]
    head_dim = local_mix // local_heads
    groups_here = local_state // SSM_STATE
    repeat = local_heads // groups_here
    blocks = length // SCAN_BLOCK
    step_size = jax.nn.softplus(step_raw + step_bias)
    log_decay = -jnp.exp(decay_log) * step_size + decay_extra
    value_heads = head_value.astype(jnp.float32).reshape(length, local_heads, head_dim)
    value_blocks = value_heads.reshape(blocks, SCAN_BLOCK, local_heads, head_dim)
    key_blocks = jnp.repeat(
        key_vectors.astype(jnp.float32).reshape(length, groups_here, SSM_STATE), repeat, axis=1
    ).reshape(blocks, SCAN_BLOCK, local_heads, SSM_STATE)
    read_blocks = jnp.repeat(
        read_vectors.astype(jnp.float32).reshape(length, groups_here, SSM_STATE), repeat, axis=1
    ).reshape(blocks, SCAN_BLOCK, local_heads, SSM_STATE)
    step_blocks = step_size.reshape(blocks, SCAN_BLOCK, local_heads)
    running_decay = jnp.cumsum(log_decay.reshape(blocks, SCAN_BLOCK, local_heads), axis=1)
    lower = jnp.arange(SCAN_BLOCK)[:, None] >= jnp.arange(SCAN_BLOCK)[None, :]
    gaps = jnp.where(
        lower[None, :, :, None],
        running_decay[:, :, None, :] - running_decay[:, None, :, :],
        -jnp.inf,
    )
    weights = jnp.einsum("blhn,bshn->blsh", read_blocks, key_blocks, precision=HIGH) * jnp.exp(gaps)
    scaled_value = value_blocks * step_blocks[..., None]
    inner = jnp.einsum("blsh,bshp->blhp", weights, scaled_value, precision=HIGH)
    block_ends = running_decay[:, -1, :]
    trailing = jnp.exp(block_ends[:, None, :] - running_decay)
    fresh = jnp.einsum("bshn,bsh,bshp->bhpn", key_blocks, trailing, scaled_value, precision=HIGH)

    def advance(carry, inputs):
        block_decay, block_state = inputs
        return (carry * block_decay[:, None, None] + block_state, carry)

    local_total, prefix = lax.scan(
        advance,
        jnp.zeros((local_heads, head_dim, SSM_STATE), jnp.float32),
        (jnp.exp(block_ends), fresh),
    )
    offsets = jnp.cumsum(block_ends, axis=0) - block_ends
    device_decay = jnp.exp(offsets[-1] + block_ends[-1])
    incoming_decay, incoming = carried_in(
        (device_decay, local_total),
        "sp",
        combine_states,
        (jnp.ones_like(device_decay), jnp.zeros_like(local_total)),
    )
    from_device = running_decay + offsets[:, None, :]
    local_off = (
        jnp.einsum("blhn,bhpn->blhp", read_blocks, prefix, precision=HIGH)
        * jnp.exp(running_decay)[..., None]
    )
    far_off = (
        jnp.einsum("blhn,hpn->blhp", read_blocks, incoming, precision=HIGH)
        * jnp.exp(from_device)[..., None]
    )
    scan_out = (inner + local_off + far_off).reshape(length, local_heads, head_dim) + skip_scale[
        None, :, None
    ] * value_heads
    gated = scan_out.reshape(length, local_mix) * jax.nn.silu(gate_in.astype(jnp.float32))
    gate_squares = lax.psum(jnp.sum(gated * gated, axis=-1), "tp")
    state_out = (gated * lax.rsqrt(gate_squares / MIX_W + EPSILON)[:, None] * state_gain).astype(
        jnp.bfloat16
    )
    branch_rows = jnp.concatenate([pool_out, state_out], axis=1)
    out_weight = jnp.concatenate([out_pool_weight, out_state_weight], axis=0)
    terms = jnp.dot(
        branch_rows,
        lax.all_gather(out_weight, "sp", axis=1, tiled=True),
        preferred_element_type=jnp.float32,
    )
    result = lax.psum_scatter(terms, "tp", scatter_dimension=1, tiled=True)
    return result.astype(jnp.bfloat16)


def solution(mesh):
    placed = (
        P("sp", "tp"),
        P("tp"),
        P("sp", "tp"),
        P("sp", "tp"),
        P("sp", "tp"),
        P("sp", "tp"),
        P("sp", "tp"),
        P("sp", "tp"),
        P("tp", None, None),
        P("tp"),
        P(None, "tp"),
        P(None, "tp"),
        P(None, "tp"),
        P("tp"),
        P("tp"),
        P("sp", "tp"),
        P("tp"),
        P("tp"),
        P("tp", "sp"),
        P("tp", "sp"),
    )
    return jax.shard_map(
        local, mesh=mesh, in_specs=placed, out_specs=P("sp", "tp"), check_vma=False
    )
```

profile of v0, /device:TPU:0, one launch (start us, length us, event | category | flops | bytes accessed | tf_op | source)
XLA Modules:
  0.0 262.7 jit_solution(2948103364905407184)
XLA Ops:
  6.6 0.7 all-gather.7.cloned.1.call-update
  7.4 0.9 copy.40
  8.2 0.9 copy.41
  9.1 0.8 copy.42
  10.0 1.8 concatenate.21
  11.9 0.7 pad_maximum_fusion
  12.7 0.6 iota_compare_fusion
  13.3 6.2 %all-gather.1 = bf16[4,1,512]{2,1,0:T(2,128)(2,1)S(1)} all-gather(bf16[1,1,512]{2,1,0:T(2,128)(2,1)S(1)} %reshape.74), channel_id=1, replica_groups=mesh['sp'=8,'tp'=4] {'tp'}, dimensions={0}, use_global_device_ids=true | all-gather | bytes 5120 | tf_op jit(solution)/shard_map/all_gather | solution.py:82
  19.5 0.1 pad_maximum_fusion.1
  19.7 0.1 mul.206
  19.7 0.7 mul.207
  20.4 0.6 add_minimum_fusion
  21.0 13.2 %all-gather.7.cloned.1.call-done = bf16[512,2048]{1,0:T(8,128)(2,1)} async-done(((bf16[512,512]{1,0:T(8,128)(2,1)}), bf16[512,2048]{1,0:T(8,128)(2,1)}) %all-gather.7.cloned.1.call-update) | async-done | bytes 2097168 | tf_op jit(solution)/shard_map/all_gather | solution.py:81
  34.3 2.2 fusion.1
  36.5 72.7 %all-gather.9.cloned.1.call-done = bf16[2048,900]{1,0:T(8,128)(2,1)} async-done(((bf16[256,900]{1,0:T(8,128)(2,1)}), bf16[2048,900]{1,0:T(8,128)(2,1)}) %all-gather.9.cloned.1.call-update) | async-done | bytes 3686416 | tf_op jit(solution)/shard_map/all_gather | solution.py:79
  109.2 4.5 %fusion.57 = (bf16[512,900]{0,1:T(8,128)(2,1)S(1)}, f32[512,900]{0,1:T(8,128)S(1)}) fusion(bf16[2048,900]{1,0:T(8,128)(2,1)} %all-gather.9.cloned.1.call-done, bf16[512,2048]{1,0:T(8,128)(2,1)S(1)} %copy-done.1, f32[2048]{0:T(1024)S(1)} %bitcast.113, f32[512]{0:T(512)S(1)} %add_rsqrt_fusion.1), kind=kOutput, calls=%fused_computation.113 | convolution fusion | flops 1892091904 | bytes 8558592 | tf_op jit(solution)/shard_map/dot_general | solution.py:90
  113.8 0.1 slice.152
  113.9 2.5 collective-permute-start.1
  116.4 0.1 fusion.52
  116.5 0.1 copy.60
  116.6 0.3 reduce_window_sum.24
  117.0 0.1 fusion.55
  117.1 0.7 copy.48
  117.9 0.7 slice.139
  118.6 0.1 copy.50
  118.7 0.7 copy.52
  119.4 0.7 copy.57
  120.1 4.6 %collective-permute-start = (bf16[15,256]{0,1:T(8,128)(2,1)}, bf16[15,256]{0,1:T(8,128)(2,1)}, u32[]{:S(2)}, u32[]{:S(2)}) collective-permute-start(bf16[15,256]{0,1:T(8,128)(2,1)} %slice.139), channel_id=1, source_target_pairs={{0,4},{4,8},{8,12},{12,16},{16,20},{20,24},{24,28},{1,5},{5,9},{9,... | collective-permute-start | bytes 23048 | tf_op jit(solution)/shard_map/ppermute | solution.py:19
  124.7 16.9 %all-gather.2 = f32[8,1,4]{2,1,0:T(1,128)} all-gather(f32[1,1,4]{2,1,0:T(1,128)S(1)} %fusion.49), channel_id=1, replica_groups=mesh['sp'=8,'tp'=4] {'sp'}, dimensions={0}, use_global_device_ids=true | all-gather | bytes 144 | tf_op jit(solution)/shard_map/all_gather | solution.py:24
  141.6 0.2 maximum_convert_fusion
  141.8 0.9 multiply_convert_fusion
  142.8 0.2 reshape_reshape.2
  143.1 0.6 copy-done.2
  143.7 0.9 fusion.32
  144.6 3.1 %while.26 = (s32[]{:T(128)}, f32[4,64,64]{2,1,0:T(8,128)S(1)}, f32[4,4,64,64]{3,2,1,0:T(8,128)}, f32[4,4]{1,0:T(4,128)S(1)}, f32[4,4,64,64]{3,2,1,0:T(8,128)S(1)}, /*index=5*/s32[]{:T(128)}, s32[]{:T(128)}) while((s32[]{:T(128)}, f32[4,64,64]{2,1,0:T(8,128)S(1)}, f32[4,4,64,64]{3,2,1,0:T(8,128)}, f32[4,4]{1,0:T(4,128)S(1)}, ...), condition=%wide.region_3.4_spmd.clone, body=%wide.region_2.3_spmd.clone.sunk | while | flops 65539 | bytes 393872 | solution.py:164
  144.7 0.7 bitcast_dynamic-update-slice_fusion.2
  145.3 0.1 bitcast_add_fusion.6
  145.4 0.7 bitcast_dynamic-update-slice_fusion.2
  146.1 0.1 bitcast_add_fusion.6
  146.2 0.7 bitcast_dynamic-update-slice_fusion.2
  146.9 0.1 bitcast_add_fusion.6
  147.0 0.7 bitcast_dynamic-update-slice_fusion.2
  147.7 0.1 bitcast_add_fusion.6
  147.8 34.8 %all-gather = f32[32,64,64]{2,1,0:T(8,128)S(1)} all-gather(f32[4,64,64]{2,1,0:T(8,128)S(1)} %get-tuple-element.78), channel_id=2, replica_groups=mesh['sp'=8,'tp'=4] {'sp'}, dimensions={0}, use_global_device_ids=true | all-gather | bytes 589824 | tf_op jit(solution)/shard_map/all_gather | solution.py:24
  182.6 0.2 while.25
  182.8 1.3 fusion.12
  184.1 1.6 fusion.11
  185.7 2.9 %fusion.8 = f32[4,128,128,4]{2,1,3,0:T(8,128)S(1)} fusion(f32[4,128,4]{1,2,0:T(4,128)} %copy.48, pred[128,128]{1,0:T(8,128)(4,1)} %iota_compare_fusion, f32[4,128,64]{1,2,0:T(8,128)S(1)} %get-tuple-element.147, f32[4,128,64]{1,2,0:T(8,128)} %copy-done.2), kind=kOutput, calls=%fused_computation.19 | convolution fusion | flops 202113024 | bytes 1335296 | tf_op jit(solution)/shard_map/blhn,bshn->blsh/dot_general | solution.py:153
  188.7 2.2 fusion.10
  190.8 0.3 copy.58
  191.2 0.3 multiply_reduce_fusion
  191.5 5.7 %psum.7 = f32[512]{0:T(512)S(1)} all-reduce(f32[512]{0:T(512)S(1)} %get-tuple-element.132), channel_id=1, replica_groups=mesh['sp'=8,'tp'=4] {'tp'}, use_global_device_ids=true, to_apply=%region_8.9 | all-reduce | flops 512 | bytes 4096 | tf_op jit(solution)/shard_map/psum | solution.py:190
  197.1 0.1 multiply_convert_fusion.1
  197.3 1.0 maximum_convert_fusion.1
  198.3 0.2 slice_add_fusion.2
  198.5 0.2 slice_add_fusion.1
  198.8 0.2 slice_add_fusion
  199.0 0.2 slice_bitcast_fusion.2
  199.2 0.3 slice_bitcast_fusion
  199.6 0.1 copy-done.10
  199.7 0.4 fusion.13
  200.1 4.8 %fusion.28 = f32[512,2048]{1,0:T(8,128)} fusion(bf16[512,2048]{1,0:T(8,128)(2,1)} %all-gather.11.cloned.1.call-done, bf16[512,256]{0,1:T(8,128)(2,1)S(1)} %multiply_convert_fusion.1, bf16[512,256]{0,1:T(8,128)(2,1)S(1)} %fusion.13), kind=kOutput, calls=%fused_computation.57 | convolution fusion | flops 1074790400 | bytes 6815744 | tf_op jit(solution)/shard_map/dot_general | solution.py:196
  205.0 49.1 %reduce-scatter.2.cloned.1.call-done = f32[512,512]{1,0:T(8,128)} async-done(((f32[512,2048]{1,0:T(8,128)}), f32[512,512]{1,0:T(8,128)}) %reduce-scatter.2.cloned.1.call-update) | async-done | bytes 1048592 | tf_op jit(solution)/shard_map/reduce_scatter | solution.py:201
  254.1 2.1 convert_element_type.70
  (65 shorter events, 0.6 us)
Async XLA Ops:
  6.5 193.0 %copy-start = (bf16[1,256,256]{2,1,0:T(8,128)(2,1)S(1)}, bf16[1,256,256]{2,1,0:T(8,128)(2,1)}, u32[]{:S(2)}) copy-start(bf16[1,256,256]{2,1,0:T(8,128)(2,1)} %param.32) | copy-start | bytes 393220
  6.5 5.3 %copy-start.4 = (bf16[256,256]{1,0:T(8,128)(2,1)S(1)}, bf16[256,256]{1,0:T(8,128)(2,1)}, u32[]{:S(2)}) copy-start(bf16[256,256]{1,0:T(8,128)(2,1)} %param.42) | copy-start | bytes 393220
  6.5 5.3 %copy-start.3 = (bf16[256,256]{1,0:T(8,128)(2,1)S(1)}, bf16[256,256]{1,0:T(8,128)(2,1)}, u32[]{:S(2)}) copy-start(bf16[256,256]{1,0:T(8,128)(2,1)} %param.43) | copy-start | bytes 393220
  6.5 6.8 %copy-start.12 = (bf16[512]{0:T(512)(128)(2,1)S(1)}, bf16[512]{0:T(512)(128)(2,1)}, u32[]{:S(2)}) copy-start(bf16[512]{0:T(512)(128)(2,1)} %param.25) | copy-start | bytes 3076
  6.5 12.9 %copy-start.6 = (f32[4,256]{1,0:T(4,128)S(1)}, f32[4,256]{1,0:T(4,128)}, u32[]{:S(2)}) copy-start(f32[4,256]{1,0:T(4,128)} %param.34) | copy-start | bytes 12292
  6.5 12.9 %copy-start.9 = (f32[4,64]{1,0:T(4,128)S(1)}, f32[4,64]{1,0:T(4,128)}, u32[]{:S(2)}) copy-start(f32[4,64]{1,0:T(4,128)} %param.35) | copy-start | bytes 3076
  6.6 12.9 %copy-start.8 = (f32[4,64]{1,0:T(4,128)S(1)}, f32[4,64]{1,0:T(4,128)}, u32[]{:S(2)}) copy-start(f32[4,64]{1,0:T(4,128)} %param.36) | copy-start | bytes 3076
  6.6 13.1 %copy-start.16 = (f32[4]{0:T(128)S(1)}, f32[4]{0:T(128)}, u32[]{:S(2)}) copy-start(f32[4]{0:T(128)} %param.38) | copy-start | bytes 52
  6.6 13.1 %copy-start.14 = (f32[4]{0:T(128)S(1)}, f32[4]{0:T(128)}, u32[]{:S(2)}) copy-start(f32[4]{0:T(128)} %param.40) | copy-start | bytes 52
  6.6 27.7 %all-gather.7.cloned.1.call-start = ((), (), s32[]{:S(2)}) async-start(), calls=%async_computation.1 | async-start | bytes 2621440 | tf_op jit(solution)/shard_map/all_gather | solution.py:81
  7.3 101.9 %all-gather.9.cloned.1.call-start = ((), (), s32[]{:S(2)}) async-start(), calls=%async_computation.2 | async-start | bytes 4718592 | tf_op jit(solution)/shard_map/all_gather | solution.py:79
  11.8 188.3 %all-gather.11.cloned.1.call-start = ((), (), s32[]{:S(2)}) async-start(), calls=%async_computation.3 | async-start | bytes 2359296 | tf_op jit(solution)/shard_map/all_gather | solution.py:198
  12.6 241.4 %reduce-scatter.2.cloned.1.call-start = ((), (), s32[]{:S(2)}) async-start(), calls=%async_computation.4 | async-start | bytes 5242880 | tf_op jit(solution)/shard_map/reduce_scatter | solution.py:201
  34.3 75.0 %copy-start.1 = (bf16[512,2048]{1,0:T(8,128)(2,1)S(1)}, bf16[512,2048]{1,0:T(8,128)(2,1)}, u32[]{:S(2)}) copy-start(bf16[512,2048]{1,0:T(8,128)(2,1)} %all-gather.7.cloned.1.call-done) | copy-start | bytes 6291460
  109.2 7.1 %copy-start.5 = (f32[512,4]{0,1:T(4,128)S(1)}, f32[512,4]{0,1:T(4,128)}, u32[]{:S(2)}) copy-start(f32[512,4]{0,1:T(4,128)} %param.39) | copy-start | bytes 24580
  109.2 7.1 %copy-start.13 = (f32[4]{0:T(128)S(1)}, f32[4]{0:T(128)}, u32[]{:S(2)}) copy-start(f32[4]{0:T(128)} %param.37) | copy-start | bytes 52
  113.9 27.7 %collective-permute-start.1 = (bf16[3,384]{0,1:T(8,128)(2,1)S(1)}, bf16[3,384]{0,1:T(8,128)(2,1)S(1)}, u32[]{:S(2)}, u32[]{:S(2)}) collective-permute-start(bf16[3,384]{0,1:T(8,128)(2,1)S(1)} %slice.152), channel_id=1, source_target_pairs={{0,4},{4,8},{8,12},{12,16},{16,20},{20,24},{24,28},{1,5},{5,9},{9,... | collective-permute-start | bytes 6920 | tf_op jit(solution)/shard_map/ppermute | solution.py:19
  120.1 77.1 %collective-permute-start = (bf16[15,256]{0,1:T(8,128)(2,1)}, bf16[15,256]{0,1:T(8,128)(2,1)}, u32[]{:S(2)}, u32[]{:S(2)}) collective-permute-start(bf16[15,256]{0,1:T(8,128)(2,1)} %slice.139), channel_id=1, source_target_pairs={{0,4},{4,8},{8,12},{12,16},{16,20},{20,24},{24,28},{1,5},{5,9},{9,... | collective-permute-start | bytes 23048 | tf_op jit(solution)/shard_map/ppermute | solution.py:19
  143.0 0.7 copy-start.2
  188.6 2.5 copy-start.7
  190.8 6.3 %copy-start.11 = (f32[256]{0:T(256)S(1)}, f32[256]{0:T(256)}, u32[]{:S(2)}) copy-start(f32[256]{0:T(256)} %param.41) | copy-start | bytes 3076
  199.0 0.7 copy-start.10
  199.0 0.7 copy-start.15
Sparse Core Ops, SparseCore 0:
  9.0 25.2 all-gather.6
  36.4 72.7 all-gather.8
  111.3 60.4 all-gather.10
  205.1 48.9 reduce-scatter.1
where the time goes:
time: 263 us
  waiting for transfers between devices  136 us (52%)
  blocking collectives  63.5 us (24%)
  matrix products  18.7 us (7%)
  between operations  13.6 us (5%)
  other arithmetic  13.4 us (5%)
  local copies, waits for them, and re-layouts  10.1 us (4%)
  starting transfers between devices  7.23 us (3%)
    all_gather x1, waiting for transfers between devices, local(): in_weight = lax.all_gather(joined, 'sp', axis=0, tiled=True)  72.7 us
    all_gather x2, blocking collectives, carried_in(): gathered = jax.tree.map(lambda a: lax.all_gather(a, axis), part)  51.7 us
    reduce_scatter x1, waiting for transfers between devices, local(): result = lax.psum_scatter(terms, 'tp', scatter_dimension=1, tiled=True)  49.1 us
    all_gather x1, waiting for transfers between devices, local(): lax.all_gather(activations, 'tp', axis=1, tiled=True)  13.2 us
    ppermute x2, starting transfers between devices, shifted(): lax.ppermute(value, axis, [(source, source + steps) for source in range(l...  7.07 us
    all_gather x1, blocking collectives, local(): lax.all_gather(norm_gain, 'tp', axis=0, tiled=True)  6.15 us
    psum x1, blocking collectives, local(): gate_squares = lax.psum(jnp.sum(gated * gated, axis=-1), 'tp')  5.66 us
  transfers between devices with their start and end apart: 6, of which 3 were waited for; matrix products, arithmetic and copies ran while one was open for 13% of the time, Pallas kernels for 0%

commit v1 on v0

--- a/solution.py
+++ b/solution.py
@@ -1,6 +1,10 @@
+import functools
+
 import jax
 import jax.numpy as jnp
 from jax import lax
+from jax.experimental import pallas as pl
+from jax.experimental.pallas import tpu as pltpu
 from jax.sharding import PartitionSpec as P
 
 SSM_STATE = 64
@@ -202,6 +206,446 @@
     return result.astype(jnp.bfloat16)
 
 
+BF = jnp.bfloat16
+F32 = jnp.float32
+MESH = pl.DeviceIdType.MESH
+
+
+def flip(index, mask):
+    bit = 1
+    while bit <= mask:
+        if mask & bit:
+            index = index + bit - 2 * bit * lax.rem(lax.div(index, bit), 2)
+        bit *= 2
+    return index
+
+
+def low_bit(mask):
+    return mask & -mask
+
+
+def spread(size):
+    bits = [1 << k for k in reversed(range(size.bit_length() - 1))]
+    order, held = [], [0]
+    for bit in bits:
+        fresh = [mask | bit for mask in held]
+        order += fresh
+        held += fresh
+    return bits, order
+
+
+def bt(a, b, **kw):
+    return lax.dot_general(a, b, (((1,), (1,)), ((), ())), preferred_element_type=F32, **kw)
+
+
+def halves(x):
+    top = x.astype(BF)
+    return top, (x - top.astype(F32)).astype(BF)
+
+
+def mixer_kernel(
+    S, T,
+    act, gain, pool_w, gate_w, value_w, key_w, read_w, step_t, mix, scale, taps_v, taps_k, taps_r,
+    head_par, extra_t, skip, sgain, opool, ostate,
+    out,
+    wbuf, sbuf, obuf, abuf, nbuf, acc, sacc, ext, conv, hsend, hrecv, scan, xs, xr, ssend, srecv,
+    brow, psend, precv, pown, qsend, qrecv, expd,
+    w_ss, w_rs, s_ss, s_rs, o_ss, o_rs, a_ss, a_rs, h_ss, h_rs, x_ss, x_rs, q_ss, q_rs, p_ss, p_rs, r_ss, r_rs,
+):
+    n, da = act.shape
+    kd = pool_w.shape[0]
+    cw = pool_w.shape[1]
+    st = key_w.shape[1]
+    ncol = wbuf.shape[2]
+    blk = SCAN_BLOCK
+    blocks = n // blk
+    hd = SSM_STATE
+    me = lax.axis_index("sp")
+    tp = lax.axis_index("tp")
+    sp_bits, sp_order = spread(S)
+    tp_bits, tp_order = spread(T)
+
+    wbuf[me, :, 0:cw] = pool_w[...]
+    wbuf[me, :, cw : 2 * cw] = gate_w[...]
+    wbuf[me, :, 2 * cw : 3 * cw] = value_w[...]
+    wbuf[me, :, 3 * cw : 3 * cw + st] = key_w[...]
+    wbuf[me, :, 3 * cw + st :] = read_w[...]
+    sbuf[me] = step_t[...]
+    abuf[tp, 0:n, :] = act[...]
+    abuf[tp, n : n + 16, :] = jnp.broadcast_to(gain[...].astype(F32), (16, da)).astype(BF)
+
+    barrier = pltpu.get_barrier_semaphore()
+    for k in range(1, S):
+        pl.semaphore_signal(barrier, inc=1, device_id={"sp": lax.rem(me + k, S)}, device_id_type=MESH)
+    for k in range(1, T):
+        pl.semaphore_signal(barrier, inc=1, device_id={"tp": lax.rem(tp + k, T)}, device_id_type=MESH)
+    obuf[me, 0:cw, :] = opool[...]
+    obuf[me, cw:, :] = ostate[...]
+    pl.semaphore_wait(barrier, S - 1 + T - 1)
+
+    started = []
+
+    def remote(src, dst, ss, rs, **peer):
+        c = pltpu.make_async_remote_copy(
+            src_ref=src, dst_ref=dst, send_sem=ss, recv_sem=rs, device_id=peer, device_id_type=MESH
+        )
+        return c
+
+    def send(*a, **k):
+        c = remote(*a, **k)
+        c.start()
+        started.append(c)
+
+    def send_block(buf, ss, rs, mask, bit, axis):
+        place = me if axis == "sp" else tp
+        i = flip(place, mask)
+        send(buf.at[i], buf.at[i], ss.at[mask | bit], rs.at[mask | bit], **{axis: flip(place, bit)})
+
+    def arrive(buf, ss, rs, mask, axis):
+        place = me if axis == "sp" else tp
+        i = flip(place, mask)
+        remote(buf.at[i], buf.at[i], ss.at[mask], rs.at[mask], **{axis: flip(place, low_bit(mask))}).wait_recv()
+
+    def push(axis, mask, *trios):
+        bits = sp_bits if axis == "sp" else tp_bits
+        for bit in bits:
+            if mask == 0 or bit < low_bit(mask):
+                for buf, ss, rs in trios:
+                    send_block(buf, ss, rs, mask, bit, axis)
+
+    W = (wbuf, w_ss, w_rs)
+    ST = (sbuf, s_ss, s_rs)
+    O = (obuf, o_ss, o_rs)
+    A = (abuf, a_ss, a_rs)
+    push("tp", 0, A)
+    push("sp", 0, W, ST)
+    for mask in tp_order:
+        arrive(*A, mask, "tp")
+        push("tp", mask, A)
+
+    def got(mask):
+        arrive(*W, mask, "sp")
+        arrive(*ST, mask, "sp")
+        push("sp", mask, W, ST)
+
+    got(sp_order[0])
+    per = da // kd
+    rt = 64
+
+    def norm_rows(i, _):
+        r = pl.ds(pl.multiple_of(i * rt, rt), rt)
+        parts = [abuf[t, r, :].astype(F32) for t in range(T)]
+        tot = sum(jnp.sum(p * p, axis=-1, keepdims=True) for p in parts)
+        rs = lax.rsqrt(tot / (da * T) + EPSILON)
+        for t in range(T):
+            g = abuf[t, n : n + 1, :].astype(F32)
+            v = (parts[t] * rs * g).astype(BF)
+            for j in range(per):
+                nbuf[t * per + j, r, :] = v[:, j * kd : (j + 1) * kd]
+        return 0
+
+    lax.fori_loop(0, n // rt, norm_rows, 0)
+    mt = 256
+
+    def add_chunk(i, first):
+        for r0 in range(0, n, mt):
+            x = nbuf[i, r0 : r0 + mt, :]
+            d = jnp.dot(x, wbuf[i], preferred_element_type=F32)
+            if first:
+                acc[r0 : r0 + mt, :] = d
+            else:
+                acc[r0 : r0 + mt, :] += d
+        d = bt(sbuf[i], nbuf[i])
+        if first:
+            sacc[...] = d
+        else:
+            sacc[...] += d
+
+    add_chunk(me, True)
+    add_chunk(flip(me, sp_order[0]), False)
+    for k, mask in enumerate(sp_order[1:]):
+        got(mask)
+        add_chunk(flip(me, mask), False)
+        if mask == sp_order[S // 2 - 2]:
+            push("sp", 0, O)
+
+    raw0 = 16
+    ccol = ncol - cw
+    hsend[:, 0:cw] = acc[n - raw0 :, 0:cw].astype(BF)
+    hsend[:, cw:] = acc[n - raw0 :, 2 * cw :].astype(BF)
+
+    def halo():
+        return remote(hsend, hrecv, h_ss, h_rs, sp=lax.rem(me + 1, S))
+
+    @pl.when(me < S - 1)
+    def _():
+        halo().start()
+
+    ext[raw0:, 0:cw] = acc[:, 0:cw].astype(BF).astype(F32)
+    ext[raw0:, cw:] = acc[:, 2 * cw :].astype(BF).astype(F32)
+    step = sacc[...] + head_par[:, 0:1]
+    step = jnp.maximum(step, 0.0) + jnp.log1p(jnp.exp(-jnp.abs(step)))
+    ld = head_par[:, 1:2] * step + extra_t[...]
+    hp = ld.shape[0]
+    r_i = lax.broadcasted_iota(jnp.int32, (blk, blk), 0)
+    c_i = lax.broadcasted_iota(jnp.int32, (blk, blk), 1)
+    upper = jnp.where(r_i <= c_i, 1.0, 0.0).astype(F32)
+    eye = jnp.where(r_i == c_i, 1.0, 0.0).astype(F32)
+    lower = r_i >= c_i
+    expand = jnp.where(
+        lax.broadcasted_iota(jnp.int32, (hp, cw), 1) // hd == lax.broadcasted_iota(jnp.int32, (hp, cw), 0), 1.0, 0.0
+    ).astype(F32)
+    eye_st = jnp.where(
+        lax.broadcasted_iota(jnp.int32, (st, st), 0) == lax.broadcasted_iota(jnp.int32, (st, st), 1), 1.0, 0.0
+    ).astype(BF)
+    cum_rs, cum_cs, st_rs, wexps = [], [], [], []
+    for b in range(blocks):
+        cols = slice(b * blk, (b + 1) * blk)
+        cum_r = jnp.dot(ld[:, cols], upper, precision=HIGH, preferred_element_type=F32)
+        st_r = step[:, cols]
+        turned = bt(eye, jnp.concatenate([cum_r, st_r], axis=0), precision=HIGH)
+        cum_c = turned[:, 0:hp]
+        w_c = jnp.exp(cum_c[blk - 1 : blk, :] - cum_c) * turned[:, hp:]
+        both = jnp.dot(
+            jnp.concatenate([w_c, jnp.exp(cum_c)], axis=0), expand, precision=HIGH, preferred_element_type=F32
+        )
+        expd[cols, :] = both[blk:, :]
+        wexps.append(both[:blk, :])
+        cum_rs.append(cum_r)
+        cum_cs.append(cum_c)
+        st_rs.append(st_r)
+
+    @pl.when(me > 0)
+    def _():
+        halo().wait_recv()
+        ext[0:raw0, :] = hrecv[...].astype(F32)
+
+    @pl.when(me == 0)
+    def _():
+        ext[0:raw0, :] = jnp.zeros((raw0, ext.shape[1]), F32)
+
+    width = taps_v.shape[0]
+    for b in range(blocks):
+        for taps, lo, hi in ((taps_v, 0, cw), (taps_k, cw, cw + st), (taps_r, cw + st, cw + 2 * st)):
+            total = jnp.zeros((blk, hi - lo), F32)
+            for k in range(width):
+                o = b * blk + raw0 - (width - 1) + k
+                total = total + taps[k : k + 1, :] * ext[o : o + blk, cw + lo : cw + hi]
+            conv[b * blk : (b + 1) * blk, lo:hi] = (total * jax.nn.sigmoid(total)).astype(BF)
+
+    run = jnp.zeros((st, cw), F32)
+    dec = jnp.ones((1, cw), F32)
+    pres, offs = [], []
+    for b in range(blocks):
+        rows = slice(b * blk, (b + 1) * blk)
+        key_t = bt(eye_st, conv[rows, cw : cw + st]).astype(BF)
+        sv = conv[rows, 0:cw].astype(F32) * wexps[b]
+        top, low = halves(sv)
+        new = jnp.dot(key_t, top, preferred_element_type=F32) + jnp.dot(key_t, low, preferred_element_type=F32)
+        bd = expd[(b + 1) * blk - 1 : (b + 1) * blk, :]
+        pres.append(run)
+        offs.append(dec)
+        run = run * bd + new
+        dec = dec * bd
+
+    in_s = jnp.zeros((st, cw), F32)
+    in_d = jnp.ones((1, cw), F32)
+    rounds = [1 << k for k in range(S.bit_length() - 1)]
+
+    def inner(b):
+        rows = slice(b * blk, (b + 1) * blk)
+        g = bt(conv[rows, cw + st :], conv[rows, cw : cw + st])
+        for h in range(cw // hd):
+            gap = jnp.where(lower, cum_cs[b][:, h : h + 1] - cum_rs[b][h : h + 1, :], -jnp.inf)
+            wm = g * jnp.exp(gap) * st_rs[b][h : h + 1, :]
+            top, low = halves(wm)
+            v = conv[rows, h * hd : (h + 1) * hd]
+            scan[rows, h * hd : (h + 1) * hd] = jnp.dot(top, v, preferred_element_type=F32) + jnp.dot(
+                low, v, preferred_element_type=F32
+            )
+
+    window = lax.shift_left(jnp.int32(2), tp)
+    back = (
+        lax.broadcasted_iota(jnp.int32, (blk, blk + raw0), 0)
+        + raw0
+        - lax.broadcasted_iota(jnp.int32, (blk, blk + raw0), 1)
+    )
+    band = jnp.where((back >= 0) & (back < window), 1.0, 0.0).astype(BF)
+
+    def pool(b):
+        rows = slice(b * blk, (b + 1) * blk)
+        sums = jnp.dot(band, ext[b * blk : (b + 1) * blk + raw0, 0:cw].astype(BF), preferred_element_type=F32)
+        pos = (me * n + b * blk + lax.broadcasted_iota(jnp.int32, (blk, cw), 0)).astype(F32)
+        counts = jnp.minimum(pos + 1.0, window.astype(F32))
+        pooled = (sums / counts - ext[b * blk + raw0 : (b + 1) * blk + raw0, 0:cw]).astype(BF)
+        brow[rows, 0:cw] = (jnp.dot(pooled, mix[0], preferred_element_type=F32) * scale[...]).astype(BF)
+
+    work = [functools.partial(inner, b) for b in range(blocks)] + [functools.partial(pool, b) for b in range(blocks)]
+    share = -(-len(work) // len(rounds))
+    o_left = list(sp_order)
+
+    def take_o(count):
+        for mask in o_left[:count]:
+            arrive(*O, mask, "sp")
+            push("sp", mask, O)
+        del o_left[:count]
+
+    for r, bit in enumerate(rounds):
+        xs[r, 0:st, :] = run
+        xs[r, st:, :] = jnp.broadcast_to(dec, (xs.shape[1] - st, cw))
+        send(xs.at[r], xr.at[r], x_ss.at[r], x_rs.at[r], sp=flip(me, bit))
+        for f in work[r * share : (r + 1) * share]:
+            f()
+        take_o(1)
+        remote(xs.at[r], xr.at[r], x_ss.at[r], x_rs.at[r], sp=flip(me, bit)).wait_recv()
+        other, odec = xr[r, 0:st, :], xr[r, st : st + 1, :]
+        later = lax.rem(lax.div(me, bit), 2) == 1
+        in_s = jnp.where(later, other * in_d + in_s, in_s)
+        in_d = jnp.where(later, odec * in_d, in_d)
+        run = jnp.where(later, other * dec + run, run * odec + other)
+        dec = dec * odec
+
+    for b in range(blocks):
+        rows = slice(b * blk, (b + 1) * blk)
+        top, low = halves(pres[b] + offs[b] * in_s)
+        rd = conv[rows, cw + st :]
+        carried = jnp.dot(rd, top, preferred_element_type=F32) + jnp.dot(rd, low, preferred_element_type=F32)
+        y = scan[rows, :] + carried * expd[rows, :] + skip[...] * conv[rows, 0:cw].astype(F32)
+        gt = acc[rows, cw : 2 * cw].astype(BF).astype(F32)
+        gated = y * (gt * jax.nn.sigmoid(gt))
+        ssend[:, rows] = bt(jnp.ones((8, cw), F32), gated * gated, precision=HIGH)
+        brow[rows, cw:] = (gated * sgain[...]).astype(BF)
+    for k in range(1, T):
+        send(ssend, srecv.at[k - 1], q_ss.at[k - 1], q_rs.at[k - 1], tp=flip(tp, k))
+    take_o(len(o_left))
+    for k in range(1, T):
+        remote(ssend, srecv.at[k - 1], q_ss.at[k - 1], q_rs.at[k - 1], tp=flip(tp, k)).wait_recv()
+    sq = ssend[...]
+    for k in range(1, T):
+        sq = sq + srecv[k - 1]
+    rs_row = lax.rsqrt(sq / (cw * T) + EPSILON)
+    rs_cols = [bt(eye, rs_row[:, b * blk : (b + 1) * blk], precision=HIGH)[:, 0:1] for b in range(blocks)]
+    wide = S // T
+    oc = obuf.shape[2]
+    parts = 2
+    pr = n // parts
+
+    def product(t, part, store):
+        rows = slice(part * pr, (part + 1) * pr)
+        rs = jnp.concatenate(rs_cols[part * blocks // parts : (part + 1) * blocks // parts], axis=0)
+        for j in range(wide):
+            i = t * wide + j
+            p = jnp.dot(brow[rows, 0:cw], obuf[i, 0:cw, :], preferred_element_type=F32)
+            p = p + rs * jnp.dot(brow[rows, cw:], obuf[i, cw:, :], preferred_element_type=F32)
+            store(rows, slice(j * oc, (j + 1) * oc), p)
+
+    def into(ref, *lead):
+        def store(rows, cols, p):
+            ref[lead + (rows, cols)] = p.astype(ref.dtype)
+        return store
+
+    near = flip(tp, 1)
+
+    def near_copy(k, part):
+        rows = pl.ds(part * pr, pr)
+        i = k * parts + part
+        return remote(psend.at[k, rows], precv.at[k, rows], p_ss.at[i], p_rs.at[i], tp=near)
+
+    def far_copy(part):
+        rows = pl.ds(part * pr, pr)
+        return remote(qsend.at[rows], qrecv.at[rows], r_ss.at[part], r_rs.at[part], tp=flip(tp, 2))
+
+    for part in range(parts):
+        product(flip(tp, 3), part, into(psend, 0))
+        near_copy(0, part).start()
+    for part in range(parts):
+        rows = slice(part * pr, (part + 1) * pr)
+        product(flip(tp, 2), part, into(pown))
+        near_copy(0, part).wait_recv()
+        qsend[rows, :] = (pown[rows, :] + precv[0, rows, :]).astype(BF)
+        far_copy(part).start()
+    for part in range(parts):
+        product(near, part, into(psend, 1))
+        near_copy(1, part).start()
+    for part in range(parts):
+        product(tp, part, into(pown))
+    for part in range(parts):
+        rows = slice(part * pr, (part + 1) * pr)
+        near_copy(1, part).wait_recv()
+        far_copy(part).wait_recv()
+        out[rows, :] = (pown[rows, :] + precv[1, rows, :] + qrecv[rows, :].astype(F32)).astype(out.dtype)
+
+    for c in started:
+        c.wait_send()
+    for part in range(parts):
+        near_copy(0, part).wait_send()
+        near_copy(1, part).wait_send()
+        far_copy(part).wait_send()
+
+    @pl.when(me < S - 1)
+    def _():
+        halo().wait_send()
+
+
+def fits(S, T, shapes):
+    n, da = shapes[0]
+    kd, cw = shapes[2]
+    st = shapes[5][1]
+    oc = shapes[18][1]
+    heads = shapes[7][1]
+    return (
+        T == 4 == POOL_GROUPS and S >= T and S & (S - 1) == 0 and S <= 16 and st == SSM_STATE
+        and cw == heads * SSM_STATE and oc % 128 == 0 and kd % 128 == 0 and da % kd == 0
+        and n % (2 * SCAN_BLOCK) == 0 and cw % 128 == 0 and oc * S == da * T
+    )
+
+
+def fused(
+    S, T, activations, norm_gain, pool_weight, gate_weight, value_weight, key_weight, read_weight,
+    step_weight, pool_mix, pool_scale, taps_value, taps_key, taps_read, step_bias, decay_log,
+    decay_extra, skip_scale, state_gain, out_pool_weight, out_state_weight,
+):
+    n, da = activations.shape
+    kd, cw = pool_weight.shape
+    st = key_weight.shape[1]
+    heads = step_weight.shape[1]
+    oc = out_pool_weight.shape[1]
+    hp = 16
+    pad = lambda x: jnp.pad(x, ((0, hp - heads), (0, 0)))
+    head_par = jnp.pad(jnp.stack([step_bias, -jnp.exp(decay_log)], axis=1), ((0, hp - heads), (0, 126)))
+    args = (
+        activations, norm_gain[None, :], pool_weight, gate_weight, value_weight, key_weight, read_weight,
+        pad(step_weight.T), pool_mix, pool_scale[None, :], taps_value, taps_key, taps_read, head_par,
+        pad(decay_extra.T), jnp.repeat(skip_scale, cw // heads)[None, :], state_gain[None, :],
+        out_pool_weight, out_state_weight,
+    )
+    ncol = 3 * cw + 2 * st
+    ccol = ncol - cw
+    V = pltpu.VMEM
+    D = pltpu.SemaphoreType.DMA
+    R = S.bit_length() - 1
+    scratch = [
+        V((S, kd, ncol), BF), V((S, hp, kd), BF), V((S, 2 * cw, oc), BF), V((T, n + 16, da), BF),
+        V((S, n, kd), BF), V((n, ncol), F32), V((hp, n), F32), V((n + 16, ccol), F32),
+        V((n, cw + 2 * st), BF), V((16, ccol), BF), V((16, ccol), BF), V((n, cw), F32),
+        V((R, st + 8, cw), F32), V((R, st + 8, cw), F32), V((8, n), F32), V((T - 1, 8, n), F32),
+        V((n, 2 * cw), BF), V((2, n, da), F32), V((2, n, da), F32), V((n, da), F32),
+        V((n, da), BF), V((n, da), BF), V((n, cw), F32),
+        D((S,)), D((S,)), D((S,)), D((S,)), D((S,)), D((S,)), D((T,)), D((T,)), D, D,
+        D((R,)), D((R,)), D((T,)), D((T,)), D((4,)), D((4,)), D((2,)), D((2,)),
+    ]
+    return pl.pallas_call(
+        functools.partial(mixer_kernel, S, T),
+        out_shape=jax.ShapeDtypeStruct((n, da), BF),
+        in_specs=[pl.BlockSpec(memory_space=pltpu.VMEM)] * len(args),
+        out_specs=pl.BlockSpec(memory_space=pltpu.VMEM),
+        scratch_shapes=scratch,
+        compiler_params=pltpu.CompilerParams(
+            collective_id=0, has_side_effects=True, vmem_limit_bytes=60 * 1024 * 1024
+        ),
+    )(*args)
+
+
 def solution(mesh):
     placed = (
         P("sp", "tp"),
@@ -225,6 +669,13 @@
         P("tp", "sp"),
         P("tp", "sp"),
     )
+    S, T = mesh.shape["sp"], mesh.shape["tp"]
+
+    def chosen(*args):
+        if fits(S, T, [a.shape for a in args]):
+            return fused(S, T, *args)
+        return local(*args)
+
     return jax.shard_map(
-        local, mesh=mesh, in_specs=placed, out_specs=P("sp", "tp"), check_vma=False
-    )
+        chosen, mesh=mesh, in_specs=placed, out_specs=P("sp", "tp"), check_vma=False
+    )

time: 263 us -> 113 us (0.43)
  waiting for transfers between devices: 136 us -> 0 us
  Pallas kernels: 0 us -> 104 us
  blocking collectives: 63.5 us -> 0 us
  matrix products: 18.7 us -> 0 us
  between operations: 13.6 us -> 0.02 us
  other arithmetic: 13.4 us -> 0.68 us
  starting transfers between devices: 7.23 us -> 0 us
    pallas_call x0 -> x1, Pallas kernels: none -> 104 us  [fused(): pl.pallas_call(functools.partial(mixer_kernel, S, T), out_shape=jax.Shape...]
    all_gather x3 -> x0, waiting for transfers between devices: 86 us -> none  [the longest x1 72.7 us: local(): in_weight = lax.all_gather(joined, 'sp', axis=0, tiled=True)]
    all_gather x3 -> x0, blocking collectives: 57.8 us -> none  [the longest x2 51.7 us: carried_in(): gathered = jax.tree.map(lambda a: lax.all_gather(a, axis), part)]
    reduce_scatter x1 -> x0, waiting for transfers between devices: 49.1 us -> none  [local(): result = lax.psum_scatter(terms, 'tp', scatter_dimension=1, tiled=True)]
    dot_general x8 -> x0, matrix products: 18.7 us -> none  [the longest x1 4.82 us: local(): jnp.dot(branch_rows, lax.all_gather(out_weight, 'sp', axis=1, tiled=True)...]
    ppermute x2 -> x0, starting transfers between devices: 7.07 us -> none  [shifted(): lax.ppermute(value, axis, [(source, source + steps) for source in range(l...]
    psum x1 -> x0, blocking collectives: 5.66 us -> none  [local(): gate_squares = lax.psum(jnp.sum(gated * gated, axis=-1), 'tp')]
    convert_element_type x7 -> x0, other arithmetic: 4.39 us -> none  [the longest x1 2.08 us: local(): return result.astype(jnp.bfloat16)]
  transfers between devices with their start and end apart: 6 -> 0, of which waited for: 3 -> 0; matrix products, arithmetic and copies ran while one was open for 13% -> 0% of each run, Pallas kernels for 0% -> 0%
where the time goes in v1:
time: 113 us
  Pallas kernels  104 us (92%)
  local copies, waits for them, and re-layouts  7.92 us (7%)
    pallas_call x1, Pallas kernels, fused(): pl.pallas_call(functools.partial(mixer_kernel, S, T), out_shape=jax.Shape...  104 us
    unnamed x19, local copies, waits for them, and re-layouts  5.23 us

profile of v1, /device:TPU:0, one launch (start us, length us, event | category | flops | bytes accessed | tf_op | source)
XLA Modules:
  0.0 112.8 jit_solution(11436762999934044261)
XLA Ops:
  0.0 0.0 copy-start.7
  0.0 0.7 copy-done.7
  0.7 0.0 copy-start.4
  0.7 0.1 copy.22
  0.8 0.6 copy-done.4
  1.3 0.0 copy-start.5
  1.3 0.6 broadcast_in_dim.12.gain
  1.9 0.1 copy-done.5
  2.0 0.0 copy-start.6
  2.0 0.1 copy.21
  2.1 0.6 copy-done.6
  2.7 0.1 broadcast_in_dim.14
  2.7 0.0 copy-start.3
  2.7 0.0 copy-start.2
  2.7 0.7 broadcast_in_dim_reshape.3.skip
  3.4 0.0 copy-start
  3.4 0.7 select_maximum_fusion.head_par
  4.1 0.0 copy-done.3
  4.1 0.6 pad.12.step_t
  4.7 0.0 copy-done.2
  4.7 0.6 pad.14.extra_t
  5.3 0.0 copy-done
  5.3 0.0 copy-start.1
  5.3 0.7 copy.23.key_w
  6.0 0.0 copy-done.1
  6.0 0.7 copy.24.read_w
  6.7 104.2 %shard_map.190 = bf16[512,512]{1,0:T(8,128)(2,1)} custom-call(bf16[512,512]{1,0:T(8,128)(2,1)} %act.1, bf16[1,512]{1,0:T(2,128)(2,1)} %broadcast_in_dim.12.gain, bf16[256,256]{1,0:T(8,128)(2,1)} %pool_w.1, bf16[256,256]{1,0:T(8,128)(2,1)} %gate_w.1, bf16[256,256]{1,0:T(8,128)(2,1)} %value_w.1, bf16[256,64]{1,0:T(8,128)(2,1)} %copy.23.key_w, ...), custom_call_target="tpu_custom_call" | custom-call | tf_op jit(solution)/shard_map/pallas_call | solution.py:637
  110.9 1.9 %copy.26 = bf16[512,512]{1,0:T(8,128)(2,1)} copy(bf16[512,512]{1,0:T(8,128)(2,1)} %shard_map.190) | data formatting | bytes 1048576
  (1 shorter events, 0.0 us)
Async XLA Ops:
  0.0 0.7 copy-start.7
  0.7 0.7 copy-start.4
  1.3 0.7 copy-start.5
  2.0 0.7 copy-start.6
  2.7 1.3 %copy-start.3 = (bf16[256,4]{0,1:T(4,128)(2,1)S(1)}, bf16[256,4]{0,1:T(4,128)(2,1)}, u32[]{:S(2)}) copy-start(bf16[256,4]{0,1:T(4,128)(2,1)} %param.27) | copy-start | bytes 6148
  2.7 1.9 %copy-start.2 = (f32[512,4]{0,1:T(4,128)S(1)}, f32[512,4]{0,1:T(4,128)}, u32[]{:S(2)}) copy-start(f32[512,4]{0,1:T(4,128)} %param.35) | copy-start | bytes 24580
  3.4 1.9 %copy-start = (bf16[256,64]{0,1:T(8,128)(2,1)S(1)}, bf16[256,64]{0,1:T(8,128)(2,1)}, u32[]{:S(2)}) copy-start(bf16[256,64]{0,1:T(8,128)(2,1)} %param.25) | copy-start | bytes 98308
  5.3 0.8 copy-start.1

commit v2 on v1

--- a/solution.py
+++ b/solution.py
@@ -220,18 +220,41 @@
     return index
 
 
-def low_bit(mask):
-    return mask & -mask
-
-
-def spread(size):
-    bits = [1 << k for k in reversed(range(size.bit_length() - 1))]
-    order, held = [], [0]
-    for bit in bits:
-        fresh = [mask | bit for mask in held]
-        order += fresh
-        held += fresh
-    return bits, order
+class Stream:
+    def __init__(self, axis, place, bits, refs, send_sems, recv_sems, base, started):
+        self.axis, self.place, self.bits, self.refs = axis, place, bits, refs
+        self.send_sems, self.recv_sems, self.base, self.started = send_sems, recv_sems, base, started
+
+    def via(self, mask):
+        return [bit for bit in self.bits if mask & bit][-1]
+
+    def copy(self, mask, bit):
+        ref = self.refs(flip(self.place, mask))
+        slot = self.base + (mask | bit)
+        return pltpu.make_async_remote_copy(
+            src_ref=ref, dst_ref=ref, send_sem=self.send_sems.at[slot], recv_sem=self.recv_sems.at[slot],
+            device_id={self.axis: flip(self.place, bit)}, device_id_type=MESH,
+        )
+
+    def push(self, mask):
+        onward = self.bits if mask == 0 else self.bits[self.bits.index(self.via(mask)) + 1 :]
+        for bit in sorted(onward):
+            c = self.copy(mask, bit)
+            c.start()
+            self.started.append(c)
+
+    def got(self, mask):
+        ref = self.refs(flip(self.place, mask))
+        slot = self.base + mask
+        pltpu.make_async_remote_copy(
+            src_ref=ref, dst_ref=ref, send_sem=self.send_sems.at[slot], recv_sem=self.recv_sems.at[slot],
+            device_id={self.axis: flip(self.place, self.via(mask))}, device_id_type=MESH,
+        ).wait_recv()
+        self.push(mask)
+
+
+def early_first(size):
+    return [m for m in range(2, size) if m // 2 & (m // 2 - 1) == 0 and m > 3]
 
 
 def bt(a, b, **kw):
@@ -246,7 +269,7 @@
 def mixer_kernel(
     S, T,
     act, gain, pool_w, gate_w, value_w, key_w, read_w, step_t, mix, scale, taps_v, taps_k, taps_r,
-    head_par, extra_t, skip, sgain, opool, ostate,
+    bias, dlog, extra_t, skip, sgain, opool, ostate,
     out,
     wbuf, sbuf, obuf, abuf, nbuf, acc, sacc, ext, conv, hsend, hrecv, scan, xs, xr, ssend, srecv,
     brow, psend, precv, pown, qsend, qrecv, expd,
@@ -255,22 +278,26 @@
     n, da = act.shape
     kd = pool_w.shape[0]
     cw = pool_w.shape[1]
-    st = key_w.shape[1]
+    st = key_w.shape[0]
     ncol = wbuf.shape[2]
     blk = SCAN_BLOCK
     blocks = n // blk
     hd = SSM_STATE
     me = lax.axis_index("sp")
     tp = lax.axis_index("tp")
-    sp_bits, sp_order = spread(S)
-    tp_bits, tp_order = spread(T)
-
     wbuf[me, :, 0:cw] = pool_w[...]
     wbuf[me, :, cw : 2 * cw] = gate_w[...]
     wbuf[me, :, 2 * cw : 3 * cw] = value_w[...]
-    wbuf[me, :, 3 * cw : 3 * cw + st] = key_w[...]
-    wbuf[me, :, 3 * cw + st :] = read_w[...]
-    sbuf[me] = step_t[...]
+    eye_kd = jnp.where(
+        lax.broadcasted_iota(jnp.int32, (kd, kd), 0) == lax.broadcasted_iota(jnp.int32, (kd, kd), 1), 1.0, 0.0
+    ).astype(BF)
+    wbuf[me, :, 3 * cw :] = bt(eye_kd, jnp.concatenate([key_w[...], read_w[...]], axis=0)).astype(BF)
+    hp = sbuf.shape[1]
+    heads = step_t.shape[0]
+    pick = jnp.where(
+        lax.broadcasted_iota(jnp.int32, (hp, heads), 0) == lax.broadcasted_iota(jnp.int32, (hp, heads), 1), 1.0, 0.0
+    ).astype(F32)
+    sbuf[me] = jnp.dot(pick.astype(BF), step_t[...], preferred_element_type=F32).astype(BF)
     abuf[tp, 0:n, :] = act[...]
     abuf[tp, n : n + 16, :] = jnp.broadcast_to(gain[...].astype(F32), (16, da)).astype(BF)
 
@@ -296,39 +323,31 @@
         c.start()
         started.append(c)
 
-    def send_block(buf, ss, rs, mask, bit, axis):
-        place = me if axis == "sp" else tp
-        i = flip(place, mask)
-        send(buf.at[i], buf.at[i], ss.at[mask | bit], rs.at[mask | bit], **{axis: flip(place, bit)})
-
-    def arrive(buf, ss, rs, mask, axis):
-        place = me if axis == "sp" else tp
-        i = flip(place, mask)
-        remote(buf.at[i], buf.at[i], ss.at[mask], rs.at[mask], **{axis: flip(place, low_bit(mask))}).wait_recv()
-
-    def push(axis, mask, *trios):
-        bits = sp_bits if axis == "sp" else tp_bits
-        for bit in bits:
-            if mask == 0 or bit < low_bit(mask):
-                for buf, ss, rs in trios:
-                    send_block(buf, ss, rs, mask, bit, axis)
-
-    W = (wbuf, w_ss, w_rs)
-    ST = (sbuf, s_ss, s_rs)
-    O = (obuf, o_ss, o_rs)
-    A = (abuf, a_ss, a_rs)
-    push("tp", 0, A)
-    push("sp", 0, W, ST)
-    for mask in tp_order:
-        arrive(*A, mask, "tp")
-        push("tp", mask, A)
-
-    def got(mask):
-        arrive(*W, mask, "sp")
-        arrive(*ST, mask, "sp")
-        push("sp", mask, W, ST)
-
-    got(sp_order[0])
+    far = [1 << k for k in reversed(range(1, S.bit_length() - 1))]
+    late = far + [1]
+    early = [1] + far
+    cut = -(-kd // 96) * 16
+    ocut = cut * 2 * cw // kd
+    wq = Stream("sp", me, late, lambda i: wbuf.at[i, pl.ds(cut, kd - cut)], w_ss, w_rs, 0, started)
+    wp = Stream("sp", me, early, lambda i: wbuf.at[i, pl.ds(0, cut)], w_ss, w_rs, S, started)
+    sq_ = Stream("sp", me, late, lambda i: sbuf.at[i], s_ss, s_rs, 0, started)
+    oq = Stream("sp", me, late, lambda i: obuf.at[i, pl.ds(ocut, 2 * cw - ocut)], o_ss, o_rs, 0, started)
+    op = Stream("sp", me, early, lambda i: obuf.at[i, pl.ds(0, ocut)], o_ss, o_rs, S, started)
+    aa = Stream("tp", tp, [1 << k for k in reversed(range(T.bit_length() - 1))], lambda i: abuf.at[i], a_ss, a_rs, 0, started)
+    masks = sorted(range(1, S), key=lambda m: (bin(m).count("1"), m))
+    even = [m for m in masks if m % 2 == 0]
+    odd = [m for m in masks if m % 2 == 1]
+    wp.push(0)
+    wq.push(0)
+    sq_.push(0)
+    aa.push(0)
+    wp.got(1)
+    aa.got(2)
+    wq.got(even[0])
+    sq_.got(even[0])
+    for mask in range(1, T):
+        if mask != 2:
+            aa.got(mask)
     per = da // kd
     rt = 64
 
@@ -362,12 +381,27 @@
             sacc[...] += d
 
     add_chunk(me, True)
-    add_chunk(flip(me, sp_order[0]), False)
-    for k, mask in enumerate(sp_order[1:]):
-        got(mask)
+    for k, mask in enumerate(even):
+        if k:
+            wq.got(mask)
+            sq_.got(mask)
+        if k == 1:
+            for m in early_first(S):
+                wp.got(m)
+        if k == len(even) - 1:
+            op.push(0)
+            oq.push(0)
+    rest = [m for m in masks if m != 1 and m not in early_first(S)]
+    for mask in even:
+        if mask in rest:
+            wp.got(mask)
         add_chunk(flip(me, mask), False)
-        if mask == sp_order[S // 2 - 2]:
-            push("sp", 0, O)
+    for mask in odd:
+        if mask in rest:
+            wp.got(mask)
+        wq.got(mask)
+        sq_.got(mask)
+        add_chunk(flip(me, mask), False)
 
     raw0 = 16
     ccol = ncol - cw
@@ -383,10 +417,13 @@
 
     ext[raw0:, 0:cw] = acc[:, 0:cw].astype(BF).astype(F32)
     ext[raw0:, cw:] = acc[:, 2 * cw :].astype(BF).astype(F32)
-    step = sacc[...] + head_par[:, 0:1]
+
+    def column(row):
+        return bt(pick, jnp.broadcast_to(row[...], (8, heads)), precision=HIGH)[:, 0:1]
+
+    step = sacc[...] + column(bias)
     step = jnp.maximum(step, 0.0) + jnp.log1p(jnp.exp(-jnp.abs(step)))
-    ld = head_par[:, 1:2] * step + extra_t[...]
-    hp = ld.shape[0]
+    ld = -jnp.exp(column(dlog)) * step + jnp.dot(pick, extra_t[...], precision=HIGH, preferred_element_type=F32)
     r_i = lax.broadcasted_iota(jnp.int32, (blk, blk), 0)
     c_i = lax.broadcasted_iota(jnp.int32, (blk, blk), 1)
     upper = jnp.where(r_i <= c_i, 1.0, 0.0).astype(F32)
@@ -395,6 +432,9 @@
     expand = jnp.where(
         lax.broadcasted_iota(jnp.int32, (hp, cw), 1) // hd == lax.broadcasted_iota(jnp.int32, (hp, cw), 0), 1.0, 0.0
     ).astype(F32)
+    skips = jnp.dot(
+        jnp.broadcast_to(skip[...], (8, heads)), expand[0:heads, :], precision=HIGH, preferred_element_type=F32
+    )[0:1, :]
     eye_st = jnp.where(
         lax.broadcasted_iota(jnp.int32, (st, st), 0) == lax.broadcasted_iota(jnp.int32, (st, st), 1), 1.0, 0.0
     ).astype(BF)
@@ -482,12 +522,13 @@
 
     work = [functools.partial(inner, b) for b in range(blocks)] + [functools.partial(pool, b) for b in range(blocks)]
     share = -(-len(work) // len(rounds))
-    o_left = list(sp_order)
+    o_left = [(op, 1), (oq, even[0])] + [(op, m) for m in early_first(S)] + [(oq, m) for m in even[1:]]
+    o_step = -(-len(o_left) // len(rounds))
+    o_rest = [(op, m) for m in masks if (op, m) not in o_left] + [(oq, m) for m in odd]
 
     def take_o(count):
-        for mask in o_left[:count]:
-            arrive(*O, mask, "sp")
-            push("sp", mask, O)
+        for stream, mask in o_left[:count]:
+            stream.got(mask)
         del o_left[:count]
 
     for r, bit in enumerate(rounds):
@@ -496,7 +537,7 @@
         send(xs.at[r], xr.at[r], x_ss.at[r], x_rs.at[r], sp=flip(me, bit))
         for f in work[r * share : (r + 1) * share]:
             f()
-        take_o(1)
+        take_o(o_step)
         remote(xs.at[r], xr.at[r], x_ss.at[r], x_rs.at[r], sp=flip(me, bit)).wait_recv()
         other, odec = xr[r, 0:st, :], xr[r, st : st + 1, :]
         later = lax.rem(lax.div(me, bit), 2) == 1
@@ -510,7 +551,7 @@
         top, low = halves(pres[b] + offs[b] * in_s)
         rd = conv[rows, cw + st :]
         carried = jnp.dot(rd, top, preferred_element_type=F32) + jnp.dot(rd, low, preferred_element_type=F32)
-        y = scan[rows, :] + carried * expd[rows, :] + skip[...] * conv[rows, 0:cw].astype(F32)
+        y = scan[rows, :] + carried * expd[rows, :] + skips * conv[rows, 0:cw].astype(F32)
         gt = acc[rows, cw : 2 * cw].astype(BF).astype(F32)
         gated = y * (gt * jax.nn.sigmoid(gt))
         ssend[:, rows] = bt(jnp.ones((8, cw), F32), gated * gated, precision=HIGH)
@@ -518,6 +559,8 @@
     for k in range(1, T):
         send(ssend, srecv.at[k - 1], q_ss.at[k - 1], q_rs.at[k - 1], tp=flip(tp, k))
     take_o(len(o_left))
+    for stream, mask in o_rest:
+        stream.got(mask)
     for k in range(1, T):
         remote(ssend, srecv.at[k - 1], q_ss.at[k - 1], q_rs.at[k - 1], tp=flip(tp, k)).wait_recv()
     sq = ssend[...]
@@ -527,7 +570,7 @@
     rs_cols = [bt(eye, rs_row[:, b * blk : (b + 1) * blk], precision=HIGH)[:, 0:1] for b in range(blocks)]
     wide = S // T
     oc = obuf.shape[2]
-    parts = 2
+    parts = 4
     pr = n // parts
 
     def product(t, part, store):
@@ -595,7 +638,8 @@
     heads = shapes[7][1]
     return (
         T == 4 == POOL_GROUPS and S >= T and S & (S - 1) == 0 and S <= 16 and st == SSM_STATE
-        and cw == heads * SSM_STATE and oc % 128 == 0 and kd % 128 == 0 and da % kd == 0
+        and cw == heads * SSM_STATE and n % (4 * SCAN_BLOCK) == 0
+        and -(-kd // 96) * 2 * cw % kd == 0 and oc % 128 == 0 and kd % 128 == 0 and da % kd == 0
         and n % (2 * SCAN_BLOCK) == 0 and cw % 128 == 0 and oc * S == da * T
     )
 
@@ -611,12 +655,10 @@
     heads = step_weight.shape[1]
     oc = out_pool_weight.shape[1]
     hp = 16
-    pad = lambda x: jnp.pad(x, ((0, hp - heads), (0, 0)))
-    head_par = jnp.pad(jnp.stack([step_bias, -jnp.exp(decay_log)], axis=1), ((0, hp - heads), (0, 126)))
     args = (
-        activations, norm_gain[None, :], pool_weight, gate_weight, value_weight, key_weight, read_weight,
-        pad(step_weight.T), pool_mix, pool_scale[None, :], taps_value, taps_key, taps_read, head_par,
-        pad(decay_extra.T), jnp.repeat(skip_scale, cw // heads)[None, :], state_gain[None, :],
+        activations, norm_gain[None, :], pool_weight, gate_weight, value_weight, key_weight.T, read_weight.T,
+        step_weight.T, pool_mix, pool_scale[None, :], taps_value, taps_key, taps_read, step_bias[None, :], decay_log[None, :],
+        decay_extra.T, skip_scale[None, :], state_gain[None, :],
         out_pool_weight, out_state_weight,
     )
     ncol = 3 * cw + 2 * st
@@ -631,8 +673,8 @@
         V((R, st + 8, cw), F32), V((R, st + 8, cw), F32), V((8, n), F32), V((T - 1, 8, n), F32),
         V((n, 2 * cw), BF), V((2, n, da), F32), V((2, n, da), F32), V((n, da), F32),
         V((n, da), BF), V((n, da), BF), V((n, cw), F32),
-        D((S,)), D((S,)), D((S,)), D((S,)), D((S,)), D((S,)), D((T,)), D((T,)), D, D,
-        D((R,)), D((R,)), D((T,)), D((T,)), D((4,)), D((4,)), D((2,)), D((2,)),
+        D((2 * S,)), D((2 * S,)), D((S,)), D((S,)), D((2 * S,)), D((2 * S,)), D((T,)), D((T,)), D, D,
+        D((R,)), D((R,)), D((T,)), D((T,)), D((8,)), D((8,)), D((4,)), D((4,)),
     ]
     return pl.pallas_call(
         functools.partial(mixer_kernel, S, T),

time: 113 us -> 102 us (0.903)
  Pallas kernels: 104 us -> 98.9 us
  local copies, waits for them, and re-layouts: 7.92 us -> 3.13 us
    pallas_call x1, Pallas kernels: 104 us -> 98.9 us  [fused(): pl.pallas_call(functools.partial(mixer_kernel, S, T), out_shape=jax.Shape...]
    unnamed x19 -> x3, local copies, waits for them, and re-layouts: 5.23 us -> 2.55 us
    pad x2 -> x0, local copies, waits for them, and re-layouts: 1.19 us -> none  [fused(): pad = lambda x: jnp.pad(x, ((0, hp - heads), (0, 0)))]
where the time goes in v2:
time: 102 us
  Pallas kernels  98.9 us (97%)
  local copies, waits for them, and re-layouts  3.13 us (3%)
    pallas_call x1, Pallas kernels, fused(): pl.pallas_call(functools.partial(mixer_kernel, S, T), out_shape=jax.Shape...  98.9 us
    unnamed x3, local copies, waits for them, and re-layouts  2.55 us

profile of v2, /device:TPU:0, one launch (start us, length us, event | category | flops | bytes accessed | tf_op | source)
XLA Modules:
  0.0 102.0 jit_solution(14737168095461935028)
XLA Ops:
  0.0 0.0 copy-start
  0.0 0.7 copy-done
  0.7 0.6 broadcast_in_dim.18.gain
  1.3 98.9 %shard_map.190 = bf16[512,512]{1,0:T(8,128)(2,1)} custom-call(bf16[512,512]{1,0:T(8,128)(2,1)} %act.1, bf16[1,512]{1,0:T(2,128)(2,1)} %broadcast_in_dim.18.gain, bf16[256,256]{1,0:T(8,128)(2,1)} %pool_w.1, bf16[256,256]{1,0:T(8,128)(2,1)} %gate_w.1, bf16[256,256]{1,0:T(8,128)(2,1)} %value_w.1, bf16[64,256]{1,0:T(8,128)(2,1)} %bitcast.9, ...), custom_call_target="tpu_custom_call" | custom-call | tf_op jit(solution)/shard_map/pallas_call | solution.py:679
  100.1 1.9 %copy.22 = bf16[512,512]{1,0:T(8,128)(2,1)} copy(bf16[512,512]{1,0:T(8,128)(2,1)} %shard_map.190) | data formatting | bytes 1048576
Async XLA Ops:
  0.0 0.7 copy-start

commit v3 on v2

--- a/solution.py
+++ b/solution.py
@@ -388,7 +388,7 @@
         if k == 1:
             for m in early_first(S):
                 wp.got(m)
-        if k == len(even) - 1:
+        if k == min(1, len(even) - 1):
             op.push(0)
             oq.push(0)
     rest = [m for m in masks if m != 1 and m not in early_first(S)]
@@ -598,15 +598,16 @@
         rows = pl.ds(part * pr, pr)
         return remote(qsend.at[rows], qrecv.at[rows], r_ss.at[part], r_rs.at[part], tp=flip(tp, 2))
 
-    for part in range(parts):
-        product(flip(tp, 3), part, into(psend, 0))
-        near_copy(0, part).start()
-    for part in range(parts):
-        rows = slice(part * pr, (part + 1) * pr)
-        product(flip(tp, 2), part, into(pown))
-        near_copy(0, part).wait_recv()
-        qsend[rows, :] = (pown[rows, :] + precv[0, rows, :]).astype(BF)
-        far_copy(part).start()
+    for part in range(parts + 1):
+        if part < parts:
+            product(flip(tp, 3), part, into(psend, 0))
+            near_copy(0, part).start()
+        if part > 0:
+            rows = slice((part - 1) * pr, part * pr)
+            product(flip(tp, 2), part - 1, into(pown))
+            near_copy(0, part - 1).wait_recv()
+            qsend[rows, :] = (pown[rows, :] + precv[0, rows, :]).astype(BF)
+            far_copy(part - 1).start()
     for part in range(parts):
         product(near, part, into(psend, 1))
         near_copy(1, part).start()

time: 102 us -> 104 us (1.020)
  Pallas kernels: 98.9 us -> 101 us
    pallas_call x1, Pallas kernels: 98.9 us -> 101 us  [fused(): pl.pallas_call(functools.partial(mixer_kernel, S, T), out_shape=jax.Shape...]
where the time goes in v3:
time: 104 us
  Pallas kernels  101 us (97%)
  local copies, waits for them, and re-layouts  3.13 us (3%)
    pallas_call x1, Pallas kernels, fused(): pl.pallas_call(functools.partial(mixer_kernel, S, T), out_shape=jax.Shape...  101 us
    unnamed x3, local copies, waits for them, and re-layouts  2.55 us

profile of v3, /device:TPU:0, one launch (start us, length us, event | category | flops | bytes accessed | tf_op | source)
XLA Modules:
  0.0 104.3 jit_solution(4993135784634887601)
XLA Ops:
  0.0 0.0 copy-start
  0.0 0.7 copy-done
  0.7 0.6 broadcast_in_dim.18.gain
  1.3 101.1 %shard_map.190 = bf16[512,512]{1,0:T(8,128)(2,1)} custom-call(bf16[512,512]{1,0:T(8,128)(2,1)} %act.1, bf16[1,512]{1,0:T(2,128)(2,1)} %broadcast_in_dim.18.gain, bf16[256,256]{1,0:T(8,128)(2,1)} %pool_w.1, bf16[256,256]{1,0:T(8,128)(2,1)} %gate_w.1, bf16[256,256]{1,0:T(8,128)(2,1)} %value_w.1, bf16[64,256]{1,0:T(8,128)(2,1)} %bitcast.9, ...), custom_call_target="tpu_custom_call" | custom-call | tf_op jit(solution)/shard_map/pallas_call | solution.py:680
  102.4 1.9 %copy.22 = bf16[512,512]{1,0:T(8,128)(2,1)} copy(bf16[512,512]{1,0:T(8,128)(2,1)} %shard_map.190) | data formatting | bytes 1048576
Async XLA Ops:
  0.0 0.7 copy-start
